TPU v7x, 32 devices: a whole 2x2x4 slice. The times are simulated.
32 devices in a mesh: ep: 8 (over z, y), tp: 4 (over x, core).
Axes of the slice: x: 2, y: 2, z: 4, core: 2. Of those that a mesh axis runs over, the one named last changes fastest.
Arguments:
- outer_gate: bfloat16 [4096, 2048], P('ep', 'tp'), may hold values from -6 to 6
- inner_gate: bfloat16 [4096, 2048], P('ep', 'tp'), may hold values from -6 to 6
- conv_values: bfloat16 [4096, 2048], P('ep', 'tp'), may hold values from -6 to 6
- conv_taps: bfloat16 [3, 2048], P(None, 'tp'), may hold values from -3 to 3
- out_weight: bfloat16 [2048, 2048], P('tp'), may hold values from -0.125 to 0.125
- moe_input: bfloat16 [4096, 2048], P(('ep', 'tp')), may hold values from -6 to 6
- norm_gain: bfloat16 [2048], replicated, may hold values from 0.099609375 to 1.8984375
- gate_proj: bfloat16 [8, 2048, 1024], P('ep', None, 'tp'), may hold values from -0.125 to 0.125
- up_proj: bfloat16 [8, 2048, 1024], P('ep', None, 'tp'), may hold values from -0.125 to 0.125
- down_proj: bfloat16 [8, 1024, 2048], P('ep', 'tp'), may hold values from -0.1875 to 0.1875
- shared_gate: bfloat16 [2048, 1024], P(None, 'tp'), may hold values from -0.125 to 0.125
- shared_up: bfloat16 [2048, 1024], P(None, 'tp'), may hold values from -0.125 to 0.125
- shared_down: bfloat16 [1024, 2048], P('tp'), may hold values from -0.1875 to 0.1875
- routes: int32 [4096, 2], P('ep'), may hold values from 0 to 7, all different within a row; in each aligned block of 128 rows (0 to 127, 128 to 255, ...) at most 64 rows name the same one
- route_weight: float32 [4096, 2], P('ep'), may hold values from 0.3 to 1.5
Outputs:
- mixer_out: bfloat16 [4096, 2048], P(('ep', 'tp'))
- expert_mix: bfloat16 [4096, 2048], P(('ep', 'tp'))
Inputs may be any that keep to these rules, and one draw needn't show every extreme that they name: `routes`: each row names 2 different experts. In the 128 rows of one device no expert is named more than 64 times, and in every draw some expert is named exactly 64 times in one device's rows.
All inputs are finite; a program needn't handle non-finite values.
Results may differ from a plain program's by a relative error of at most 0.012.
Values may be sent and summed in bfloat16 or wider, within the bound.
A program may use at most 128 MiB of HBM per device.

v0:
```python
from functools import partial
import jax
import jax.numpy as jnp
from jax import lax
from jax.sharding import PartitionSpec as P

epsilon = 1e-06


def shifted(block, axis, distance):
    devices = range(lax.axis_size(axis))
    route = [(i - distance, i) for i in devices if i - distance in devices]
    return lax.ppermute(block, axis, route)


def rms_norm(inputs, scales):
    values = inputs.astype(jnp.float32)
    square = jnp.mean(values * values, axis=-1, keepdims=True)
    return (values * lax.rsqrt(square + epsilon) * scales.astype(jnp.float32)).astype(jnp.bfloat16)


def swiglu(inputs, gate_w, up_w):
    gate_term = jnp.dot(inputs, gate_w, preferred_element_type=jnp.float32)
    upward = jnp.dot(inputs, up_w, preferred_element_type=jnp.float32)
    return (jax.nn.silu(gate_term) * upward).astype(jnp.bfloat16)


def slot_table(block_routes, experts, capacity):
    flat_ids = block_routes.reshape(-1)
    onehot = (flat_ids[:, None] == jnp.arange(experts, dtype=jnp.int32)[None, :]).astype(jnp.int32)
    earlier = jnp.cumsum(onehot, axis=0) - onehot
    slot_ids = jnp.sum(earlier * onehot, axis=1)
    targets = flat_ids * capacity + slot_ids
    owners = jnp.arange(flat_ids.shape[0], dtype=jnp.int32) // block_routes.shape[1]
    sources = jnp.zeros((experts * capacity,), jnp.int32).at[targets].set(owners)
    filled = jnp.zeros((experts * capacity,), jnp.bfloat16).at[targets].set(1.0)
    return (sources, filled, targets)


def send_own(normed, own_routes, table_maker, ep_count, capacity):
    sources, filled, own_targets = table_maker(own_routes)
    outgoing = (normed[sources] * filled[:, None]).reshape(ep_count, capacity, normed.shape[1])
    landed = lax.all_to_all(outgoing, "ep", split_axis=0, concat_axis=0, tiled=True)
    return (landed, own_targets)


def per_device(
    outer_gate,
    inner_gate,
    conv_values,
    conv_taps,
    out_weight,
    moe_input,
    norm_gain,
    gate_proj,
    up_proj,
    down_proj,
    shared_gate,
    shared_up,
    shared_down,
    routes,
    route_weight,
):
    tp_count = lax.axis_size("tp")
    ep_count = lax.axis_size("ep")
    my_slot = lax.axis_index("tp")
    group_len = inner_gate.shape[0]
    mix_rows = group_len // tp_count
    channels = inner_gate.shape[1]
    model_width = moe_input.shape[1]
    own_rows = moe_input.shape[0]
    top_count = routes.shape[1]
    capacity = 2 * own_rows * top_count // ep_count
    slot_rows = ep_count * capacity
    reach_rows = conv_taps.shape[0] - 1
    edge_rows = jnp.stack(
        (inner_gate[group_len - reach_rows :], conv_values[group_len - reach_rows :])
    )
    before = shifted(edge_rows, "ep", 1)
    full_gate = jnp.concatenate((before[0], inner_gate), axis=0).astype(jnp.float32)
    full_values = jnp.concatenate((before[1], conv_values), axis=0).astype(jnp.float32)
    product = full_gate * full_values
    tap_values = conv_taps.astype(jnp.float32)
    convolved = tap_values[0] * product[0:group_len]
    for offset in range(1, reach_rows + 1):
        convolved = convolved + tap_values[offset] * product[offset : offset + group_len]
    gate_rows = (outer_gate.astype(jnp.float32) * convolved).astype(jnp.bfloat16)
    gate_rows = gate_rows.reshape(tp_count, mix_rows, channels)
    normed = rms_norm(moe_input, norm_gain)
    group_normed = lax.all_gather(normed, "tp", axis=0, tiled=True)
    group_split = group_normed.reshape(tp_count, own_rows, model_width)
    own_weights = lax.dynamic_slice_in_dim(route_weight, my_slot * own_rows, own_rows, 0)
    own_routes = lax.dynamic_slice_in_dim(routes, my_slot * own_rows, own_rows, 0)
    table_maker = partial(slot_table, experts=ep_count, capacity=capacity)
    local_routed = None
    landed, own_targets = send_own(normed, own_routes, table_maker, ep_count, capacity)
    gate_full, up_full, down_full = (
        lax.all_gather(gate_proj, "tp", axis=2, tiled=True),
        lax.all_gather(up_proj, "tp", axis=2, tiled=True),
        lax.all_gather(down_proj, "tp", axis=1, tiled=True),
    )
    hidden = swiglu(landed.reshape(slot_rows, model_width), gate_full[0], up_full[0])
    unit_block = hidden.shape[1] // tp_count
    local_routed = jnp.zeros((slot_rows, model_width), jnp.float32)
    for piece_idx in range(tp_count):
        partial_sum = jnp.dot(
            hidden[:, piece_idx * unit_block : (piece_idx + 1) * unit_block],
            down_full[0, piece_idx * unit_block : (piece_idx + 1) * unit_block],
            preferred_element_type=jnp.float32,
        ).astype(jnp.bfloat16)
        local_routed = local_routed + partial_sum.astype(jnp.float32)
    routed_rows = 0
    expert_block = routed_rows + own_rows
    joint_block = mix_rows + expert_block
    dev_count = joint_block * lax.axis_size("tp") // joint_block
    block_rows = gate_rows
    block_rows = block_rows.reshape(dev_count * mix_rows, channels)
    projected = jnp.dot(block_rows, out_weight, preferred_element_type=jnp.float32)
    shared_in = group_split
    shared_in = shared_in.reshape(dev_count * own_rows, model_width)
    shared_out = jnp.dot(
        swiglu(shared_in, shared_gate, shared_up), shared_down, preferred_element_type=jnp.float32
    )
    shared_out = shared_out.reshape(dev_count, own_rows, model_width)
    combined = jnp.concatenate(
        (projected.reshape(dev_count, mix_rows, model_width), shared_out), axis=1
    )
    summed = lax.psum_scatter(
        combined.reshape(dev_count * joint_block, model_width).astype(jnp.bfloat16),
        "tp",
        scatter_dimension=0,
        tiled=True,
    ).astype(jnp.float32)
    mixer_out = summed[:mix_rows].astype(jnp.bfloat16)
    expert_total = summed[mix_rows:]
    routed_back = local_routed.astype(jnp.bfloat16)
    routed_back = routed_back.reshape(ep_count, capacity, model_width)
    returned = lax.all_to_all(routed_back, "ep", split_axis=0, concat_axis=0, tiled=True).reshape(
        slot_rows, model_width
    )
    picked = returned[own_targets].reshape(own_rows, top_count, model_width).astype(jnp.float32)
    routed = jnp.sum(picked * own_weights[:, :, None], axis=1)
    expert_mix = (expert_total + routed).astype(jnp.bfloat16)
    return (mixer_out, expert_mix)


def solution(mesh):
    return jax.shard_map(
        per_device,
        mesh=mesh,
        in_specs=(
            P("ep", "tp"),
            P("ep", "tp"),
            P("ep", "tp"),
            P(None, "tp"),
            P("tp", None),
            P(("ep", "tp"), None),
            P(),
            P("ep", None, "tp"),
            P("ep", None, "tp"),
            P("ep", "tp", None),
            P(None, "tp"),
            P(None, "tp"),
            P("tp", None),
            P("ep", None),
            P("ep", None),
        ),
        out_specs=(P(("ep", "tp"), None), P(("ep", "tp"), None)),
        check_vma=False,
    )
```

profile of v0, /device:TPU:0, one launch (start us, length us, event | category | flops | bytes accessed | tf_op | source)
XLA Modules:
  0.0 229.2 jit_solution(8211461132235295244)
XLA Ops:
  7.2 0.8 convert_element_type.85
  8.1 1.2 fusion.7
  9.3 2.0 fusion.9
  11.4 0.7 all-gather.7.cloned.1.call-update
  13.4 0.7 broadcast_multiply_fusion.1
  15.7 1.4 scatter_custom_fusion
  17.2 3.3 %gather_fusion = bf16[512,2048]{1,0:T(8,128)(2,1)} fusion(bf16[128,2048]{1,0:T(8,128)(2,1)S(1)} %copy-done.1, s32[1024]{0:T(1024)S(1)} %pad_clamp_fusion.1), kind=kCustom, calls=%fused_computation | custom fusion | bytes 4196352 | tf_op jit(solution)/shard_map/gather | solution.py:42
  20.5 2.2 scatter_custom_fusion.1
  22.7 3.1 %broadcast_multiply_fusion = bf16[8,64,2048]{2,1,0:T(8,128)(2,1)} fusion(bf16[8,64,2048]{2,1,0:T(8,128)(2,1)} %bitcast.58, bf16[8,64]{1,0:T(8,128)(2,1)S(1)} %mul.134), kind=kLoop, calls=%fused_computation.38 | loop fusion | flops 1048576 | bytes 4195328 | tf_op jit(solution)/shard_map/mul | solution.py:42
  25.8 7.4 %all-to-all-start = ((bf16[8,64,2048]{2,1,0:T(8,128)(2,1)}), bf16[8,64,2048]{2,1,0:T(8,128)(2,1)}, u32[]{:S(2)}, u32[]{:S(2)}) async-start(bf16[8,64,2048]{2,1,0:T(8,128)(2,1)} %broadcast_multiply_fusion), calls=%async_computation.1 | async-start | bytes 4194304 | tf_op jit(solution)/shard_map/all_to_all | solution.py:43
  33.4 4.2 %collective-permute-start = (bf16[2,2,512]{2,1,0:T(2,128)(2,1)S(1)}, bf16[2,2,512]{2,1,0:T(2,128)(2,1)S(1)}, u32[]{:S(2)}, u32[]{:S(2)}) collective-permute-start(bf16[2,2,512]{2,1,0:T(2,128)(2,1)S(1)} %pad_maximum_fusion.1), channel_id=1, source_target_pairs={{0,4},{4,8},{8,12},{12,16},{16,20},{20,24},{24,28},{1,5},{5,9},{9,... | collective-permute-start | bytes 12296 | tf_op jit(solution)/shard_map/ppermute | solution.py:13
  37.6 12.8 %collective-permute-done = bf16[2,2,512]{2,1,0:T(2,128)(2,1)S(1)} collective-permute-done((bf16[2,2,512]{2,1,0:T(2,128)(2,1)S(1)}, bf16[2,2,512]{2,1,0:T(2,128)(2,1)S(1)}, u32[]{:S(2)}, u32[]{:S(2)}) %collective-permute-start) | collective-permute-done | bytes 4128 | tf_op jit(solution)/shard_map/ppermute | solution.py:13
  50.7 2.8 %convolution_convert_fusion.5 = bf16[512,2048]{1,0:T(8,128)(2,1)} fusion(bf16[512,2048]{1,0:T(8,128)(2,1)S(1)} %copy-done, f32[514,512]{1,0:T(8,128)S(1)} %convert_multiply_fusion.2, bf16[512,512]{1,0:T(8,128)(2,1)S(1)} %copy-done.7, f32[512]{0:T(512)S(1)} %bitcast.67, f32[512]{0:T(512)S(1)} %bitcast.66, f32[512]{0:T(512)S(1)} %bitcast.65), kind=kOutput, calls=%fused_computation.15 | convolution fusion | flops 1076887552 | bytes 7870464 | tf_op jit(solution)/shard_map/dot_general | solution.py:118
  53.5 3.1 %fusion.37 = f32[512,256]{1,0:T(8,128)} fusion(bf16[512,2048]{1,0:T(8,128)(2,1)} %all-gather.5.cloned.1.call-done, bf16[2048,256]{1,0:T(8,128)(2,1)S(1)} %copy-done.6), kind=kOutput, calls=%fused_computation.82 | convolution fusion | flops 536870912 | bytes 3670016 | tf_op jit(solution)/shard_map/dot_general | solution.py:23
  56.6 6.0 %convolution_convert_fusion.4 = bf16[512,2048]{1,0:T(8,128)(2,1)} fusion(bf16[256,2048]{1,0:T(8,128)(2,1)} %param.27, bf16[512,2048]{1,0:T(8,128)(2,1)} %all-gather.5.cloned.1.call-done, bf16[2048,256]{1,0:T(8,128)(2,1)} %param.26, f32[512,256]{1,0:T(8,128)} %fusion.37), kind=kOutput, calls=%fused_computation.14 | convolution fusion | flops 1075576832 | bytes 6815744 | tf_op jit(solution)/shard_map/dot_general | solution.py:121
  62.6 4.8 %pad_maximum_fusion = bf16[4,256,2048]{2,1,0:T(8,128)(2,1)} fusion(bf16[4,128,2048]{2,1,0:T(8,128)(2,1)} %bitcast.60, bf16[4,128,2048]{2,1,0:T(8,128)(2,1)} %bitcast.59), kind=kLoop, calls=%fused_computation.4 | loop fusion | flops 8388608 | bytes 8388608 | tf_op jit(solution)/shard_map/concatenate | solution.py:125
  67.4 14.2 %all-to-all-done = bf16[8,64,2048]{2,1,0:T(8,128)(2,1)} async-done(((bf16[8,64,2048]{2,1,0:T(8,128)(2,1)}), bf16[8,64,2048]{2,1,0:T(8,128)(2,1)}, u32[]{:S(2)}, u32[]{:S(2)}) %all-to-all-start) | async-done | bytes 2097184 | tf_op jit(solution)/shard_map/all_to_all | solution.py:43
  81.6 7.2 %fusion.2 = f32[512,1024]{1,0:T(8,128)} fusion(bf16[512,2048]{1,0:T(8,128)(2,1)} %bitcast.15, bf16[1,2048,1024]{2,1,0:T(8,128)(2,1)} %all-gather.7.cloned.1.call-done), kind=kOutput, calls=%fused_computation.7 | convolution fusion | flops 2147483648 | bytes 8388608 | tf_op jit(solution)/shard_map/dot_general | solution.py:23
  88.8 21.2 %all-gather.9.cloned.1.call-done = bf16[1,2048,1024]{2,1,0:T(8,128)(2,1)} async-done(((bf16[1,2048,256]{2,1,0:T(8,128)(2,1)}), bf16[1,2048,1024]{2,1,0:T(8,128)(2,1)}) %all-gather.9.cloned.1.call-update) | async-done | bytes 4194320 | tf_op jit(solution)/shard_map/all_gather | solution.py:99
  110.0 5.9 %multiply_convert_fusion = bf16[512,1024]{1,0:T(8,128)(2,1)S(1)} fusion(f32[512,1024]{1,0:T(8,128)} %fusion.2, bf16[512,2048]{1,0:T(8,128)(2,1)} %bitcast.15, bf16[1,2048,1024]{2,1,0:T(8,128)(2,1)} %all-gather.9.cloned.1.call-done), kind=kOutput, calls=%fused_computation.17 | convolution fusion | flops 2150629376 | bytes 9437184 | tf_op jit(solution)/shard_map/dot_general | solution.py:24
  115.9 30.0 %all-gather.11.cloned.1.call-done = bf16[1,1024,2048]{2,1,0:T(8,128)(2,1)} async-done(((bf16[1,256,2048]{2,1,0:T(8,128)(2,1)}), bf16[1,1024,2048]{2,1,0:T(8,128)(2,1)}) %all-gather.11.cloned.1.call-update) | async-done | bytes 4194320 | tf_op jit(solution)/shard_map/all_gather | solution.py:100
  145.9 2.1 convolution_convert_fusion
  148.0 1.9 convolution_convert_fusion.1
  149.9 0.7 convolution_convert_fusion.2
  150.6 2.6 %add_convert_fusion = bf16[512,2048]{1,0:T(8,128)(2,1)} fusion(bf16[512,2048]{1,0:T(8,128)(2,1)S(1)} %convolution_convert_fusion, bf16[512,2048]{1,0:T(8,128)(2,1)S(1)} %convolution_convert_fusion.1, bf16[512,2048]{1,0:T(8,128)(2,1)S(1)} %convolution_convert_fusion.2, bf16[1,1024,2048]{2,1,0:T(8,128)(2,1)S(1)} %copy-done.2, ...), kind=kOutput, calls=%fused_computation.9 | convolution fusion | flops 546308096 | bytes 9699328 | tf_op jit(solution)/shard_map/dot_general | solution.py:106
  153.2 5.5 %all-to-all-start.1 = ((bf16[8,64,2048]{2,1,0:T(8,128)(2,1)}), bf16[8,64,2048]{2,1,0:T(8,128)(2,1)}, u32[]{:S(2)}, u32[]{:S(2)}) async-start(bf16[8,64,2048]{2,1,0:T(8,128)(2,1)} %bitcast.57), calls=%async_computation.2 | async-start | bytes 4194304 | tf_op jit(solution)/shard_map/all_to_all | solution.py:138
  159.5 47.9 %all-to-all-done.1 = bf16[8,64,2048]{2,1,0:T(8,128)(2,1)} async-done(((bf16[8,64,2048]{2,1,0:T(8,128)(2,1)}), bf16[8,64,2048]{2,1,0:T(8,128)(2,1)}, u32[]{:S(2)}, u32[]{:S(2)}) %all-to-all-start.1) | async-done | bytes 2097184 | tf_op jit(solution)/shard_map/all_to_all | solution.py:138
  207.5 4.2 %gather_fusion.1 = bf16[256,2048]{1,0:T(8,128)(2,1)S(1)} fusion(bf16[512,2048]{1,0:T(8,128)(2,1)} %bitcast.23, s32[1024]{0:T(1024)S(1)} %pad_clamp_fusion), kind=kCustom, calls=%fused_computation.1 | custom fusion | bytes 2098176 | tf_op jit(solution)/shard_map/gather | solution.py:141
  211.7 2.4 %reshape.96 = f32[128,2,2048]{2,1,0:T(2,128)} reshape(bf16[256,2048]{1,0:T(8,128)(2,1)S(1)} %gather_fusion.1) | data formatting | bytes 3145728 | tf_op jit(solution)/shard_map/convert_element_type | solution.py:141
  214.1 4.7 %multiply_reduce_fusion = f32[128,2048]{1,0:T(8,128)S(1)} fusion(f32[128,2,2048]{2,1,0:T(2,128)} %reshape.96, f32[128,2]{1,0:T(8,128)S(1)} %copy.21), kind=kLoop, calls=%fused_computation.16 | loop fusion | flops 786432 | bytes 3146752 | tf_op jit(solution)/shard_map/reduce_sum | solution.py:142
  218.8 1.9 slice.105
  220.7 1.9 add_convert_fusion.1
  (54 shorter events, 4.3 us)
Async XLA Ops:
  7.2 43.5 %copy-start = (bf16[512,2048]{1,0:T(8,128)(2,1)S(1)}, bf16[512,2048]{1,0:T(8,128)(2,1)}, u32[]{:S(2)}) copy-start(bf16[512,2048]{1,0:T(8,128)(2,1)} %param.19) | copy-start | bytes 6291460
  7.2 46.3 %all-gather.5.cloned.1.call-start = ((), (), s32[]{:S(2)}) async-start(), calls=%async_computation.3 | async-start | bytes 2621440 | tf_op jit(solution)/shard_map/all_gather | solution.py:90
  11.3 5.8 %copy-start.1 = (bf16[128,2048]{1,0:T(8,128)(2,1)S(1)}, bf16[128,2048]{1,0:T(8,128)(2,1)}, u32[]{:S(2)}) copy-start(bf16[128,2048]{1,0:T(8,128)(2,1)} %fusion.9) | copy-start | bytes 1572868
  11.3 70.3 %all-gather.7.cloned.1.call-start = ((), (), s32[]{:S(2)}) async-start(), calls=%async_computation.5 | async-start | bytes 5242880 | tf_op jit(solution)/shard_map/all_gather | solution.py:98
  12.1 97.9 %all-gather.9.cloned.1.call-start = ((), (), s32[]{:S(2)}) async-start(), calls=%async_computation.6 | async-start | bytes 5242880 | tf_op jit(solution)/shard_map/all_gather | solution.py:99
  12.8 133.0 %all-gather.11.cloned.1.call-start = ((), (), s32[]{:S(2)}) async-start(), calls=%async_computation.7 | async-start | bytes 5242880 | tf_op jit(solution)/shard_map/all_gather | solution.py:100
  25.8 7.5 %copy-start.3 = (bf16[512,512]{1,0:T(8,128)(2,1)S(1)}, bf16[512,512]{1,0:T(8,128)(2,1)}, u32[]{:S(2)}) copy-start(bf16[512,512]{1,0:T(8,128)(2,1)} %param.16) | copy-start | bytes 1572868
  25.8 7.5 %copy-start.4 = (bf16[512,512]{1,0:T(8,128)(2,1)S(1)}, bf16[512,512]{1,0:T(8,128)(2,1)}, u32[]{:S(2)}) copy-start(bf16[512,512]{1,0:T(8,128)(2,1)} %param.17) | copy-start | bytes 1572868
  25.8 11.8 %copy-start.5 = (bf16[3,512]{1,0:T(4,128)(2,1)S(1)}, bf16[3,512]{1,0:T(4,128)(2,1)}, u32[]{:S(2)}) copy-start(bf16[3,512]{1,0:T(4,128)(2,1)} %param.18) | copy-start | bytes 9220
  25.8 55.8 %all-to-all-start = ((bf16[8,64,2048]{2,1,0:T(8,128)(2,1)}), bf16[8,64,2048]{2,1,0:T(8,128)(2,1)}, u32[]{:S(2)}, u32[]{:S(2)}) async-start(bf16[8,64,2048]{2,1,0:T(8,128)(2,1)} %broadcast_multiply_fusion), calls=%async_computation.1 | async-start | bytes 4194304 | tf_op jit(solution)/shard_map/all_to_all | solution.py:43
  33.3 185.6 %reduce-scatter.2.cloned.1.call-start = ((), (), s32[]{:S(2)}) async-start(), calls=%async_computation.4 | async-start | bytes 5242880 | tf_op jit(solution)/shard_map/reduce_scatter | solution.py:128
  33.3 17.4 %copy-start.7 = (bf16[512,512]{1,0:T(8,128)(2,1)S(1)}, bf16[512,512]{1,0:T(8,128)(2,1)}, u32[]{:S(2)}) copy-start(bf16[512,512]{1,0:T(8,128)(2,1)} %param.15) | copy-start | bytes 1572868
  33.4 17.0 %collective-permute-start = (bf16[2,2,512]{2,1,0:T(2,128)(2,1)S(1)}, bf16[2,2,512]{2,1,0:T(2,128)(2,1)S(1)}, u32[]{:S(2)}, u32[]{:S(2)}) collective-permute-start(bf16[2,2,512]{2,1,0:T(2,128)(2,1)S(1)} %pad_maximum_fusion.1), channel_id=1, source_target_pairs={{0,4},{4,8},{8,12},{12,16},{16,20},{20,24},{24,28},{1,5},{5,9},{9,... | collective-permute-start | bytes 12296 | tf_op jit(solution)/shard_map/ppermute | solution.py:13
  50.7 2.8 %copy-start.6 = (bf16[2048,256]{1,0:T(8,128)(2,1)S(1)}, bf16[2048,256]{1,0:T(8,128)(2,1)}, u32[]{:S(2)}) copy-start(bf16[2048,256]{1,0:T(8,128)(2,1)} %param.25) | copy-start | bytes 3145732
  145.9 4.0 %copy-start.2 = (bf16[1,1024,2048]{2,1,0:T(8,128)(2,1)S(1)}, bf16[1,1024,2048]{2,1,0:T(8,128)(2,1)}, u32[]{:S(2)}) copy-start(bf16[1,1024,2048]{2,1,0:T(8,128)(2,1)} %all-gather.11.cloned.1.call-done) | copy-start | bytes 12582916
  153.2 54.3 %all-to-all-start.1 = ((bf16[8,64,2048]{2,1,0:T(8,128)(2,1)}), bf16[8,64,2048]{2,1,0:T(8,128)(2,1)}, u32[]{:S(2)}, u32[]{:S(2)}) async-start(bf16[8,64,2048]{2,1,0:T(8,128)(2,1)} %bitcast.57), calls=%async_computation.2 | async-start | bytes 4194304 | tf_op jit(solution)/shard_map/all_to_all | solution.py:138
Sparse Core Ops, SparseCore 0:
  11.5 25.2 all-gather.4
  38.3 34.9 all-gather.6
  74.9 34.9 all-gather.8
  111.4 34.4 all-gather.10
  148.2 44.5 reduce-scatter.1
where the time goes:
time: 230 us; the launch traced here: 229 us
  waiting for transfers between devices  128 us (56%)
  matrix products  32.2 us (14%)
  other arithmetic  20.4 us (9%)
  starting transfers between devices  17.3 us (8%)
  local copies, waits for them, and re-layouts  17.2 us (7%)
  between operations  14 us (6%)
    all_to_all x1, waiting for transfers between devices, per_device(): lax.all_to_all(routed_back, 'ep', split_axis=0, concat_axis=0, tiled=True)  47.9 us
    all_gather x1, waiting for transfers between devices, per_device(): lax.all_gather(down_proj, 'tp', axis=1, tiled=True)  30 us
    all_gather x1, waiting for transfers between devices, per_device(): lax.all_gather(up_proj, 'tp', axis=2, tiled=True)  21.2 us
    all_to_all x1, waiting for transfers between devices, send_own(): lax.all_to_all(outgoing, 'ep', split_axis=0, concat_axis=0, tiled=True)  14.2 us
    ppermute x1, waiting for transfers between devices, shifted(): return lax.ppermute(block, axis, route)  12.8 us
    dot_general x2, matrix products, swiglu(): gate_term = jnp.dot(inputs, gate_w, preferred_element_type=jnp.float32)  10.3 us
    all_to_all x1, starting transfers between devices, send_own(): lax.all_to_all(outgoing, 'ep', split_axis=0, concat_axis=0, tiled=True)  7.44 us
    dot_general x4, matrix products, per_device(): jnp.dot(hidden[:, piece_idx * unit_block:(piece_idx + 1) * unit_block], d...  7.31 us
  transfers between devices with their start and end apart: 8, of which 5 were waited for; matrix products, arithmetic and copies ran while one was open for 27% of the time, Pallas kernels for 0%

commit v1 on v0

--- a/solution.py
+++ b/solution.py
@@ -97,7 +97,9 @@
     gate_full, up_full, down_full = (
         lax.all_gather(gate_proj, "tp", axis=2, tiled=True),
         lax.all_gather(up_proj, "tp", axis=2, tiled=True),
-        lax.all_gather(down_proj, "tp", axis=1, tiled=True),
+        jnp.concatenate(
+            lax.all_to_all(jnp.stack([down_proj] * lax.axis_size("tp")), "tp", 0, 0), axis=1
+        ),
     )
     hidden = swiglu(landed.reshape(slot_rows, model_width), gate_full[0], up_full[0])
     unit_block = hidden.shape[1] // tp_count

time: 230 us -> 240 us (1.043)
  starting transfers between devices: 17.3 us -> 22.3 us
  local copies, waits for them, and re-layouts: 17.2 us -> 19.7 us
    all_gather x1 -> x0, waiting for transfers between devices: 30 us -> none  [per_device(): lax.all_gather(down_proj, 'tp', axis=1, tiled=True)]
    all_to_all x0 -> x1, waiting for transfers between devices: none -> 22.3 us  [per_device(): lax.all_to_all(jnp.stack([down_proj] * lax.axis_size('tp')), 'tp', 0, 0)]
    all_to_all x0 -> x1, starting transfers between devices: none -> 4.93 us  [per_device(): lax.all_to_all(jnp.stack([down_proj] * lax.axis_size('tp')), 'tp', 0, 0)]
    all_gather x1, waiting for transfers between devices: 21.2 us -> 26 us  [per_device(): lax.all_gather(up_proj, 'tp', axis=2, tiled=True)]
    all_to_all x1, waiting for transfers between devices: 14.2 us -> 18.9 us  [send_own(): lax.all_to_all(outgoing, 'ep', split_axis=0, concat_axis=0, tiled=True)]
    another operation x1 -> x2, local copies, waits for them, and re-layouts: 0.01 us -> 2.56 us  [the longest x1 2.55 us: per_device(): jnp.stack([down_proj] * lax.axis_size('tp'))]
  transfers between devices with their start and end apart: 8 -> 8, of which waited for: 5 -> 5; matrix products, arithmetic and copies ran while one was open for 27% -> 28% of each run, Pallas kernels for 0% -> 0%
where the time goes in v1:
time: 240 us; the launch traced here: 239 us
  waiting for transfers between devices  129 us (54%)
  matrix products  34 us (14%)
  starting transfers between devices  22.3 us (9%)
  other arithmetic  20.4 us (8%)
  local copies, waits for them, and re-layouts  19.7 us (8%)
  between operations  14 us (6%)
    all_to_all x1, waiting for transfers between devices, per_device(): lax.all_to_all(routed_back, 'ep', split_axis=0, concat_axis=0, tiled=True)  47.4 us
    all_gather x1, waiting for transfers between devices, per_device(): lax.all_gather(up_proj, 'tp', axis=2, tiled=True)  26 us
    all_to_all x1, waiting for transfers between devices, per_device(): lax.all_to_all(jnp.stack([down_proj] * lax.axis_size('tp')), 'tp', 0, 0)  22.3 us
    all_to_all x1, waiting for transfers between devices, send_own(): lax.all_to_all(outgoing, 'ep', split_axis=0, concat_axis=0, tiled=True)  18.9 us
    ppermute x1, waiting for transfers between devices, shifted(): return lax.ppermute(block, axis, route)  13 us
    dot_general x4, matrix products, per_device(): jnp.dot(hidden[:, piece_idx * unit_block:(piece_idx + 1) * unit_block], d...  9.65 us
    dot_general x2, matrix products, swiglu(): gate_term = jnp.dot(inputs, gate_w, preferred_element_type=jnp.float32)  9.6 us
    all_to_all x1, starting transfers between devices, send_own(): lax.all_to_all(outgoing, 'ep', split_axis=0, concat_axis=0, tiled=True)  7.42 us
  transfers between devices with their start and end apart: 8, of which 5 were waited for; matrix products, arithmetic and copies ran while one was open for 28% of the time, Pallas kernels for 0%

profile of v1, /device:TPU:0, one launch (start us, length us, event | category | flops | bytes accessed | tf_op | source)
XLA Modules:
  0.0 239.4 jit_solution(7369048838931113882)
XLA Ops:
  7.2 0.8 convert_element_type.85
  8.1 1.2 fusion.7
  9.3 2.0 fusion.9
  15.1 1.4 scatter_custom_fusion
  16.6 3.3 %gather_fusion = bf16[512,2048]{1,0:T(8,128)(2,1)} fusion(bf16[128,2048]{1,0:T(8,128)(2,1)S(1)} %copy-done.1, s32[1024]{0:T(1024)S(1)} %pad_clamp_fusion.1), kind=kCustom, calls=%fused_computation | custom fusion | bytes 4196352 | tf_op jit(solution)/shard_map/gather | solution.py:42
  19.9 2.2 scatter_custom_fusion.1
  22.1 3.2 %broadcast_multiply_fusion = bf16[8,64,2048]{2,1,0:T(8,128)(2,1)} fusion(bf16[8,64,2048]{2,1,0:T(8,128)(2,1)} %bitcast.60, bf16[8,64]{1,0:T(8,128)(2,1)S(1)} %mul.134), kind=kLoop, calls=%fused_computation.38 | loop fusion | flops 1048576 | bytes 4195328 | tf_op jit(solution)/shard_map/mul | solution.py:42
  25.3 7.4 %all-to-all-start = ((bf16[8,64,2048]{2,1,0:T(8,128)(2,1)}), bf16[8,64,2048]{2,1,0:T(8,128)(2,1)}, u32[]{:S(2)}, u32[]{:S(2)}) async-start(bf16[8,64,2048]{2,1,0:T(8,128)(2,1)} %broadcast_multiply_fusion), calls=%async_computation.1 | async-start | bytes 4194304 | tf_op jit(solution)/shard_map/all_to_all | solution.py:43
  32.8 4.0 %collective-permute-start = (bf16[2,2,512]{2,1,0:T(2,128)(2,1)S(1)}, bf16[2,2,512]{2,1,0:T(2,128)(2,1)S(1)}, u32[]{:S(2)}, u32[]{:S(2)}) collective-permute-start(bf16[2,2,512]{2,1,0:T(2,128)(2,1)S(1)} %pad_maximum_fusion.1), channel_id=1, source_target_pairs={{0,4},{4,8},{8,12},{12,16},{16,20},{20,24},{24,28},{1,5},{5,9},{9,... | collective-permute-start | bytes 12296 | tf_op jit(solution)/shard_map/ppermute | solution.py:13
  36.9 13.0 %collective-permute-done = bf16[2,2,512]{2,1,0:T(2,128)(2,1)S(1)} collective-permute-done((bf16[2,2,512]{2,1,0:T(2,128)(2,1)S(1)}, bf16[2,2,512]{2,1,0:T(2,128)(2,1)S(1)}, u32[]{:S(2)}, u32[]{:S(2)}) %collective-permute-start) | collective-permute-done | bytes 4128 | tf_op jit(solution)/shard_map/ppermute | solution.py:13
  50.2 2.8 %convolution_convert_fusion.5 = bf16[512,2048]{1,0:T(8,128)(2,1)} fusion(bf16[512,2048]{1,0:T(8,128)(2,1)S(1)} %copy-done, f32[514,512]{1,0:T(8,128)S(1)} %convert_multiply_fusion.2, bf16[512,512]{1,0:T(8,128)(2,1)S(1)} %copy-done.7, f32[512]{0:T(512)S(1)} %bitcast.70, f32[512]{0:T(512)S(1)} %bitcast.69, f32[512]{0:T(512)S(1)} %bitcast.68), kind=kOutput, calls=%fused_computation.15 | convolution fusion | flops 1076887552 | bytes 7870464 | tf_op jit(solution)/shard_map/dot_general | solution.py:120
  53.0 3.1 %fusion.37 = f32[512,256]{1,0:T(8,128)} fusion(bf16[512,2048]{1,0:T(8,128)(2,1)} %all-gather.4.cloned.1.call-done, bf16[2048,256]{1,0:T(8,128)(2,1)S(1)} %copy-done.6), kind=kOutput, calls=%fused_computation.82 | convolution fusion | flops 536870912 | bytes 3670016 | tf_op jit(solution)/shard_map/dot_general | solution.py:23
  56.1 6.1 %convolution_convert_fusion.4 = bf16[512,2048]{1,0:T(8,128)(2,1)} fusion(bf16[256,2048]{1,0:T(8,128)(2,1)} %param.27, bf16[512,2048]{1,0:T(8,128)(2,1)} %all-gather.4.cloned.1.call-done, bf16[2048,256]{1,0:T(8,128)(2,1)} %param.26, f32[512,256]{1,0:T(8,128)} %fusion.37), kind=kOutput, calls=%fused_computation.14 | convolution fusion | flops 1075576832 | bytes 6815744 | tf_op jit(solution)/shard_map/dot_general | solution.py:123
  62.1 18.9 %all-to-all-done = bf16[8,64,2048]{2,1,0:T(8,128)(2,1)} async-done(((bf16[8,64,2048]{2,1,0:T(8,128)(2,1)}), bf16[8,64,2048]{2,1,0:T(8,128)(2,1)}, u32[]{:S(2)}, u32[]{:S(2)}) %all-to-all-start) | async-done | bytes 2097184 | tf_op jit(solution)/shard_map/all_to_all | solution.py:43
  81.1 2.5 %stack.19 = bf16[4,1,256,2048]{3,2,1,0:T(8,128)(2,1)} broadcast(bf16[256,2048]{1,0:T(8,128)(2,1)S(1)} %bitcast.63), dimensions={2,3} | broadcast | bytes 5242880 | tf_op jit(solution)/shard_map/stack | solution.py:101
  83.6 4.9 %all-to-all-start.1 = ((bf16[4,1,256,2048]{3,2,1,0:T(8,128)(2,1)}), bf16[4,1,256,2048]{3,2,1,0:T(8,128)(2,1)}, u32[]{:S(2)}, u32[]{:S(2)}) async-start(bf16[4,1,256,2048]{3,2,1,0:T(8,128)(2,1)} %stack.19), calls=%async_computation.2 | async-start | bytes 8388608 | tf_op jit(solution)/shard_map/all_to_all | solution.py:101
  88.8 4.8 %pad_maximum_fusion = bf16[4,256,2048]{2,1,0:T(8,128)(2,1)} fusion(bf16[4,128,2048]{2,1,0:T(8,128)(2,1)} %bitcast.62, bf16[4,128,2048]{2,1,0:T(8,128)(2,1)} %bitcast.61), kind=kLoop, calls=%fused_computation.4 | loop fusion | flops 8388608 | bytes 8388608 | tf_op jit(solution)/shard_map/concatenate | solution.py:127
  93.6 6.5 %fusion.2 = f32[512,1024]{1,0:T(8,128)} fusion(bf16[512,2048]{1,0:T(8,128)(2,1)} %bitcast.15, bf16[1,2048,1024]{2,1,0:T(8,128)(2,1)} %all-gather.6.cloned.1.call-done), kind=kOutput, calls=%fused_computation.7 | convolution fusion | flops 2147483648 | bytes 8388608 | tf_op jit(solution)/shard_map/dot_general | solution.py:23
  100.1 26.0 %all-gather.8.cloned.1.call-done = bf16[1,2048,1024]{2,1,0:T(8,128)(2,1)} async-done(((bf16[1,2048,256]{2,1,0:T(8,128)(2,1)}), bf16[1,2048,1024]{2,1,0:T(8,128)(2,1)}) %all-gather.8.cloned.1.call-update) | async-done | bytes 4194320 | tf_op jit(solution)/shard_map/all_gather | solution.py:99
  126.1 5.9 %multiply_convert_fusion = bf16[512,1024]{1,0:T(8,128)(2,1)S(1)} fusion(f32[512,1024]{1,0:T(8,128)} %fusion.2, bf16[512,2048]{1,0:T(8,128)(2,1)} %bitcast.15, bf16[1,2048,1024]{2,1,0:T(8,128)(2,1)} %all-gather.8.cloned.1.call-done), kind=kOutput, calls=%fused_computation.17 | convolution fusion | flops 2150629376 | bytes 9437184 | tf_op jit(solution)/shard_map/dot_general | solution.py:24
  132.0 22.3 %all-to-all-done.1 = bf16[4,1,256,2048]{3,2,1,0:T(8,128)(2,1)} async-done(((bf16[4,1,256,2048]{3,2,1,0:T(8,128)(2,1)}), bf16[4,1,256,2048]{3,2,1,0:T(8,128)(2,1)}, u32[]{:S(2)}, u32[]{:S(2)}) %all-to-all-start.1) | async-done | bytes 4194336 | tf_op jit(solution)/shard_map/all_to_all | solution.py:101
  154.3 1.9 convolution_convert_fusion
  156.3 1.9 convolution_convert_fusion.1
  158.2 1.9 convolution_convert_fusion.2
  160.1 3.8 %add_convert_fusion = bf16[512,2048]{1,0:T(8,128)(2,1)} fusion(bf16[512,2048]{1,0:T(8,128)(2,1)S(1)} %convolution_convert_fusion, bf16[512,2048]{1,0:T(8,128)(2,1)S(1)} %convolution_convert_fusion.1, bf16[512,2048]{1,0:T(8,128)(2,1)S(1)} %convolution_convert_fusion.2, bf16[1,1024,2048]{2,1,0:T(8,128)(2,1)} %bitcast.19, ...), kind=kOutput, calls=%fused_computation.9 | convolution fusion | flops 546308096 | bytes 9699328 | tf_op jit(solution)/shard_map/dot_general | solution.py:108
  164.0 5.5 %all-to-all-start.2 = ((bf16[8,64,2048]{2,1,0:T(8,128)(2,1)}), bf16[8,64,2048]{2,1,0:T(8,128)(2,1)}, u32[]{:S(2)}, u32[]{:S(2)}) async-start(bf16[8,64,2048]{2,1,0:T(8,128)(2,1)} %bitcast.59), calls=%async_computation.3 | async-start | bytes 4194304 | tf_op jit(solution)/shard_map/all_to_all | solution.py:140
  170.3 47.4 %all-to-all-done.2 = bf16[8,64,2048]{2,1,0:T(8,128)(2,1)} async-done(((bf16[8,64,2048]{2,1,0:T(8,128)(2,1)}), bf16[8,64,2048]{2,1,0:T(8,128)(2,1)}, u32[]{:S(2)}, u32[]{:S(2)}) %all-to-all-start.2) | async-done | bytes 2097184 | tf_op jit(solution)/shard_map/all_to_all | solution.py:140
  217.7 4.2 %gather_fusion.1 = bf16[256,2048]{1,0:T(8,128)(2,1)S(1)} fusion(bf16[512,2048]{1,0:T(8,128)(2,1)} %bitcast.25, s32[1024]{0:T(1024)S(1)} %pad_clamp_fusion), kind=kCustom, calls=%fused_computation.1 | custom fusion | bytes 2098176 | tf_op jit(solution)/shard_map/gather | solution.py:143
  221.9 2.4 reshape.103
  224.3 4.7 %multiply_reduce_fusion = f32[128,2048]{1,0:T(8,128)S(1)} fusion(f32[128,2,2048]{2,1,0:T(2,128)} %reshape.103, f32[128,2]{1,0:T(8,128)S(1)} %copy.21), kind=kLoop, calls=%fused_computation.16 | loop fusion | flops 786432 | bytes 3146752 | tf_op jit(solution)/shard_map/reduce_sum | solution.py:144
  229.1 1.9 slice.105
  230.9 1.9 add_convert_fusion.1
  (54 shorter events, 5.3 us)
Async XLA Ops:
  7.2 43.0 %copy-start = (bf16[512,2048]{1,0:T(8,128)(2,1)S(1)}, bf16[512,2048]{1,0:T(8,128)(2,1)}, u32[]{:S(2)}) copy-start(bf16[512,2048]{1,0:T(8,128)(2,1)} %param.19) | copy-start | bytes 6291460
  7.2 45.8 %all-gather.4.cloned.1.call-start = ((), (), s32[]{:S(2)}) async-start(), calls=%async_computation.4 | async-start | bytes 2621440 | tf_op jit(solution)/shard_map/all_gather | solution.py:90
  11.3 5.3 %copy-start.1 = (bf16[128,2048]{1,0:T(8,128)(2,1)S(1)}, bf16[128,2048]{1,0:T(8,128)(2,1)}, u32[]{:S(2)}) copy-start(bf16[128,2048]{1,0:T(8,128)(2,1)} %fusion.9) | copy-start | bytes 1572868
  11.3 82.3 %all-gather.6.cloned.1.call-start = ((), (), s32[]{:S(2)}) async-start(), calls=%async_computation.6 | async-start | bytes 5242880 | tf_op jit(solution)/shard_map/all_gather | solution.py:98
  12.1 114.0 %all-gather.8.cloned.1.call-start = ((), (), s32[]{:S(2)}) async-start(), calls=%async_computation.7 | async-start | bytes 5242880 | tf_op jit(solution)/shard_map/all_gather | solution.py:99
  25.3 7.4 %copy-start.3 = (bf16[512,512]{1,0:T(8,128)(2,1)S(1)}, bf16[512,512]{1,0:T(8,128)(2,1)}, u32[]{:S(2)}) copy-start(bf16[512,512]{1,0:T(8,128)(2,1)} %param.16) | copy-start | bytes 1572868
  25.3 7.4 %copy-start.4 = (bf16[512,512]{1,0:T(8,128)(2,1)S(1)}, bf16[512,512]{1,0:T(8,128)(2,1)}, u32[]{:S(2)}) copy-start(bf16[512,512]{1,0:T(8,128)(2,1)} %param.17) | copy-start | bytes 1572868
  25.3 11.5 %copy-start.5 = (bf16[3,512]{1,0:T(4,128)(2,1)S(1)}, bf16[3,512]{1,0:T(4,128)(2,1)}, u32[]{:S(2)}) copy-start(bf16[3,512]{1,0:T(4,128)(2,1)} %param.18) | copy-start | bytes 9220
  25.3 55.8 %all-to-all-start = ((bf16[8,64,2048]{2,1,0:T(8,128)(2,1)}), bf16[8,64,2048]{2,1,0:T(8,128)(2,1)}, u32[]{:S(2)}, u32[]{:S(2)}) async-start(bf16[8,64,2048]{2,1,0:T(8,128)(2,1)} %broadcast_multiply_fusion), calls=%async_computation.1 | async-start | bytes 4194304 | tf_op jit(solution)/shard_map/all_to_all | solution.py:43
  32.7 17.4 %copy-start.7 = (bf16[512,512]{1,0:T(8,128)(2,1)S(1)}, bf16[512,512]{1,0:T(8,128)(2,1)}, u32[]{:S(2)}) copy-start(bf16[512,512]{1,0:T(8,128)(2,1)} %param.15) | copy-start | bytes 1572868
  32.8 17.1 %collective-permute-start = (bf16[2,2,512]{2,1,0:T(2,128)(2,1)S(1)}, bf16[2,2,512]{2,1,0:T(2,128)(2,1)S(1)}, u32[]{:S(2)}, u32[]{:S(2)}) collective-permute-start(bf16[2,2,512]{2,1,0:T(2,128)(2,1)S(1)} %pad_maximum_fusion.1), channel_id=1, source_target_pairs={{0,4},{4,8},{8,12},{12,16},{16,20},{20,24},{24,28},{1,5},{5,9},{9,... | collective-permute-start | bytes 12296 | tf_op jit(solution)/shard_map/ppermute | solution.py:13
  50.2 2.8 %copy-start.6 = (bf16[2048,256]{1,0:T(8,128)(2,1)S(1)}, bf16[2048,256]{1,0:T(8,128)(2,1)}, u32[]{:S(2)}) copy-start(bf16[2048,256]{1,0:T(8,128)(2,1)} %param.25) | copy-start | bytes 3145732
  56.1 25.0 %copy-start.2 = (bf16[1,256,2048]{2,1,0:T(8,128)(2,1)S(1)}, bf16[1,256,2048]{2,1,0:T(8,128)(2,1)}, u32[]{:S(2)}) copy-start(bf16[1,256,2048]{2,1,0:T(8,128)(2,1)} %param.24) | copy-start | bytes 3145732
  83.6 70.7 %all-to-all-start.1 = ((bf16[4,1,256,2048]{3,2,1,0:T(8,128)(2,1)}), bf16[4,1,256,2048]{3,2,1,0:T(8,128)(2,1)}, u32[]{:S(2)}, u32[]{:S(2)}) async-start(bf16[4,1,256,2048]{3,2,1,0:T(8,128)(2,1)} %stack.19), calls=%async_computation.2 | async-start | bytes 8388608 | tf_op jit(solution)/shard_map/all_to_all | solution.py:101
  88.5 140.5 %reduce-scatter.2.cloned.1.call-start = ((), (), s32[]{:S(2)}) async-start(), calls=%async_computation.5 | async-start | bytes 5242880 | tf_op jit(solution)/shard_map/reduce_scatter | solution.py:130
  164.0 53.7 %all-to-all-start.2 = ((bf16[8,64,2048]{2,1,0:T(8,128)(2,1)}), bf16[8,64,2048]{2,1,0:T(8,128)(2,1)}, u32[]{:S(2)}, u32[]{:S(2)}) async-start(bf16[8,64,2048]{2,1,0:T(8,128)(2,1)} %bitcast.59), calls=%async_computation.3 | async-start | bytes 4194304 | tf_op jit(solution)/shard_map/all_to_all | solution.py:140
Sparse Core Ops, SparseCore 0:
  11.5 25.2 all-gather.3
  38.3 34.9 all-gather.5
  74.9 51.1 all-gather.7
  128.5 48.1 reduce-scatter.1
